TPU v7x, 32 devices: a whole 2x2x4 slice. The times are simulated.
32 devices in a mesh: sp: 8 (over z, y), tp: 4 (over x, core).
Axes of the slice: x: 2, y: 2, z: 4, core: 2. Of those that a mesh axis runs over, the one named last changes fastest.
Arguments:
- queries: bfloat16 [2048, 2048], P('sp', 'tp'), may hold values from -16 to 16
- key_value_pairs: bfloat16 [2048, 512], P('sp', 'tp'), may hold values from -16 to 16
- forget_gate_total: float32 [2048, 32], P('sp', 'tp'), may hold values from -2048 to 0, as said below
- residual_in: bfloat16 [2048, 2048], P(('sp', 'tp')), may hold values from -12 to 12
- out_weight: bfloat16 [2048, 2048], P('tp'), may hold values from -0.25 to 0.25
- norm_gain: float32 [2048], replicated, may hold values from 0.1 to 1.9
- routes: int32 [2048, 2], P(('sp', 'tp')), may hold values from 0 to 7, all different within a row; in each aligned block of 64 rows (0 to 63, 64 to 127, ...) at most 24 rows name the same one
- route_weight: float32 [2048, 2], P(('sp', 'tp')), may hold values from 0.2 to 1
- expert_gate: bfloat16 [8, 2048, 3072], P('sp', None, 'tp'), may hold values from -0.125 to 0.125
- expert_up: bfloat16 [8, 2048, 3072], P('sp', None, 'tp'), may hold values from -0.125 to 0.125
- expert_down: bfloat16 [8, 3072, 2048], P('sp', 'tp'), may hold values from -0.109375 to 0.109375
Outputs:
- layer_out: bfloat16 [2048, 2048], P(('sp', 'tp'))
Inputs may be any that keep to these rules, and one draw needn't show every extreme that they name: `routes`: each row names 2 different experts; among the rows of one device no expert is named more than 24 times, and in every draw some device names some expert exactly 24 times. `forget_gate_total`: along the positions, each head's values never rise.
All inputs are finite; a program needn't handle non-finite values.
Results may differ from a plain program's by a relative error of at most 0.011.
Values may be sent and summed in bfloat16 or wider, within the bound.
A program may use at most 64 MiB of HBM per device.

v0:
```python
import math

import jax
import jax.numpy as jnp
from jax import lax
from jax.sharding import PartitionSpec as P

HEAD_SIZE = 64


NEG_FILL = -1e30
NORM_EPS = 1e-06


def slot_ranks(chosen, experts):
    onehot = (chosen[..., None] == jnp.arange(experts, dtype=jnp.int32)).astype(jnp.int32)
    earlier = jnp.cumsum(onehot, axis=-2) - onehot
    return jnp.sum(earlier * onehot, axis=-1)


def fill_slots(source_rows, target, slot_total, per_row):
    owner_slot = (
        jnp.zeros((slot_total,), jnp.int32)
        .at[target]
        .set(jnp.arange(1, target.shape[0] + 1, dtype=jnp.int32))
    )
    picked = source_rows[jnp.maximum(owner_slot - 1, 0) // per_row]
    return jnp.where((owner_slot > 0)[:, None], picked, jnp.zeros_like(picked))


def local(
    queries,
    key_value_pairs,
    forget_gate_total,
    residual_in,
    out_weight,
    norm_gain,
    routes,
    route_weight,
    expert_gate,
    expert_up,
    expert_down,
):
    seq_devices = lax.axis_size("sp")
    head_devices = lax.axis_size("tp")
    tok_rows = queries.shape[0]
    local_heads = queries.shape[1] // HEAD_SIZE
    local_groups = key_value_pairs.shape[1] // (2 * HEAD_SIZE)
    queries_per_group = local_heads // local_groups
    score_scale = HEAD_SIZE ** (-0.5)
    seq_index = lax.axis_index("sp")
    own_start = seq_index * tok_rows
    all_gates = lax.all_gather(forget_gate_total, "sp", axis=0, tiled=True)

    def attend_block(carried, query_set, kv_block, key_start):
        grouped_queries, query_gate, query_pos = query_set
        run_max, run_total, run_acc = carried
        key_count = kv_block.shape[0]
        key_value_head_list = kv_block.reshape(key_count, local_groups, 2 * HEAD_SIZE)
        scores = (
            jnp.einsum(
                "tkgd,skd->ktgs",
                grouped_queries,
                key_value_head_list[:, :, :HEAD_SIZE],
                preferred_element_type=jnp.float32,
            )
            * score_scale
        )
        gate_block = lax.dynamic_slice_in_dim(all_gates, key_start, key_count, 0)
        key_gate = gate_block.reshape(key_count, local_groups, queries_per_group).transpose(1, 2, 0)
        scores = scores + query_gate[..., None] - key_gate[:, None, :, :]
        key_pos = key_start + jnp.arange(key_count, dtype=jnp.int32)
        scores = jnp.where(
            key_pos[None, None, None, :] <= query_pos[None, :, None, None], scores, NEG_FILL
        )
        new_max = jnp.maximum(run_max, jnp.max(scores, axis=3))
        weights = jnp.exp(scores - new_max[..., None])
        rescale = jnp.exp(run_max - new_max)
        run_total = run_total * rescale + jnp.sum(weights, axis=3)
        block_sum = jnp.einsum(
            "ktgs,skd->ktgd",
            weights.astype(jnp.bfloat16),
            key_value_head_list[:, :, HEAD_SIZE:],
            preferred_element_type=jnp.float32,
        )
        return (new_max, run_total, run_acc * rescale[..., None] + block_sum)

    def start_state(row_count):
        return (
            jnp.full((local_groups, row_count, queries_per_group), NEG_FILL, jnp.float32),
            jnp.zeros((local_groups, row_count, queries_per_group), jnp.float32),
            jnp.zeros((local_groups, row_count, queries_per_group, HEAD_SIZE), jnp.float32),
        )

    row_count = queries.shape[0]
    grouped_queries = queries.reshape(row_count, local_groups, queries_per_group, HEAD_SIZE)
    query_gate = lax.dynamic_slice_in_dim(all_gates, own_start, row_count, 0)
    query_gate = query_gate.reshape(row_count, local_groups, queries_per_group).transpose(1, 0, 2)
    query_pos = own_start + jnp.arange(row_count, dtype=jnp.int32)
    query_sets = ((grouped_queries, query_gate, query_pos),)
    initial = tuple((start_state(query_set[2].shape[0]) for query_set in query_sets))
    kv_piece = lax.all_gather(key_value_pairs, "sp", axis=0, tiled=True)
    length = kv_piece.shape[0]
    key_block = math.gcd(length, 512)
    kv_blocks = kv_piece.reshape(length // key_block, key_block, kv_piece.shape[1])

    def one_block(block_index, inner_states):
        key_start = block_index * key_block
        updated = []
        for query_set, running in zip(query_sets, inner_states):
            last_pos = query_set[2][-1]
            updated.append(
                lax.cond(
                    key_start <= last_pos,
                    lambda state, chosen_set=query_set: attend_block(
                        state, chosen_set, kv_blocks[block_index], key_start
                    ),
                    lambda state: state,
                    running,
                )
            )
        return tuple(updated)

    states = lax.fori_loop(0, length // key_block, one_block, initial)
    run_max, run_total, run_acc = states[0]
    row_count = run_total.shape[1]
    attended = (
        (run_acc / run_total[..., None])
        .transpose(1, 0, 2, 3)
        .reshape(row_count, local_heads * HEAD_SIZE)
        .astype(jnp.bfloat16)
    )
    own_rows = tok_rows // head_devices
    row_block = attended
    mixed_rows = lax.psum_scatter(
        jnp.dot(row_block, out_weight, preferred_element_type=jnp.float32).astype(jnp.bfloat16),
        "tp",
        scatter_dimension=0,
        tiled=True,
    ).astype(jnp.float32)
    hidden_state = residual_in.astype(jnp.float32) + mixed_rows
    normed = (
        hidden_state
        * lax.rsqrt(jnp.mean(hidden_state * hidden_state, axis=1, keepdims=True) + NORM_EPS)
        * norm_gain
    ).astype(jnp.bfloat16)
    top_count = routes.shape[1]
    capacity = max(2, 3 * own_rows * top_count // (2 * seq_devices))
    model_width = normed.shape[1]
    chosen = routes.reshape(-1)
    target = chosen * capacity + slot_ranks(chosen, seq_devices)
    outgoing = fill_slots(normed, target, seq_devices * capacity, top_count).reshape(
        seq_devices, capacity, model_width
    )
    incoming = lax.all_to_all(outgoing, "sp", split_axis=0, concat_axis=0, tiled=True)
    arrived = lax.all_gather(incoming, "tp", axis=0, tiled=True)
    flat_in = arrived.reshape(-1, model_width)
    gate_value = jnp.dot(flat_in, expert_gate[0], preferred_element_type=jnp.float32)
    up_value = jnp.dot(flat_in, expert_up[0], preferred_element_type=jnp.float32)
    hidden_rows = (
        (jax.nn.silu(gate_value) * up_value)
        .astype(jnp.bfloat16)
        .reshape(arrived.shape[0], capacity, -1)
    )
    row_block = hidden_rows
    summed = lax.psum_scatter(
        jnp.einsum(
            "rcf,fd->rcd", row_block, expert_down[0], preferred_element_type=jnp.float32
        ).astype(jnp.bfloat16),
        "tp",
        scatter_dimension=0,
        tiled=True,
    )
    returned = lax.all_to_all(summed, "sp", split_axis=0, concat_axis=0, tiled=True)
    picked = returned.reshape(-1, model_width)[target].reshape(own_rows, top_count, model_width)
    combined = jnp.sum(picked.astype(jnp.float32) * route_weight[..., None], axis=1)
    return (hidden_state + combined).astype(jnp.bfloat16)


def solution(mesh):
    return jax.shard_map(
        local,
        mesh=mesh,
        in_specs=(
            P("sp", "tp"),
            P("sp", "tp"),
            P("sp", "tp"),
            P(("sp", "tp"), None),
            P("tp", None),
            P(),
            P(("sp", "tp"), None),
            P(("sp", "tp"), None),
            P("sp", None, "tp"),
            P("sp", None, "tp"),
            P("sp", "tp", None),
        ),
        out_specs=P(("sp", "tp"), None),
        check_vma=False,
    )
```

profile of v0, /device:TPU:0, one launch (start us, length us, event | category | flops | bytes accessed | tf_op | source)
XLA Modules:
  0.0 288.9 jit_solution(7621068759620404694)
XLA Ops:
  6.5 32.7 %all_gather.10 = f32[2048,8]{0,1:T(8,128)S(1)} all-gather(f32[256,8]{0,1:T(8,128)} %param.17), channel_id=1, replica_groups=mesh['sp'=8,'tp'=4] {'sp'}, dimensions={0}, use_global_device_ids=true | all-gather | bytes 73728 | tf_op jit(solution)/shard_map/all_gather | solution.py:53
  39.2 33.6 %all_gather.9 = bf16[2048,128]{1,0:T(8,128)(2,1)} all-gather(bf16[256,128]{1,0:T(8,128)(2,1)} %param.16), channel_id=1, replica_groups=mesh['sp'=8,'tp'=4] {'sp'}, dimensions={0}, use_global_device_ids=true | all-gather | bytes 589824 | tf_op jit(solution)/shard_map/all_gather | solution.py:102
  72.8 2.0 copy.25
  74.8 1.8 copy.24
  77.4 10.9 %while.17 = (s32[]{:T(128)}, f32[1,256,8]{1,2,0:T(8,128)S(1)}, f32[1,256,8]{1,2,0:T(8,128)S(1)}, f32[1,256,8,64]{1,3,2,0:T(8,128)}, s32[256]{0:T(256)S(1)}, /*in...) while((s32[]{:T(128)}, f32[1,256,8]{1,2,0:T(8,128)S(1)}, ...), condition=%wide.region_5.6_spmd, body=%wide.region_0.5_spmd.sunk | while | flops 286661120 | bytes 19248544 | solution.py:124
  78.6 6.3 %conditional.2 = ((f32[1,256,8]{1,2,0:T(8,128)S(1)}, f32[1,256,8]{1,2,0:T(8,128)S(1)}, f32[1,256,8,64]{1,3,2,0:T(8,128)})) conditional(s32[]{:T(128)} %convert_element_type.90, (f32[1,256,8]{1,2,0:T(8,128)S(1)}, f32[1,256,8]{1,2,0:T(8,128)S(1)}, f32[1,256,8,64]{1,3,2,0:T(8,128)}) %tuple.41, (s32[]{:T(128)}, s32[256]{0:T(256)S(1)}, s32[]{:T(128)}, ...), branch_computations={%region_1.0_spmd, %region_2.4_spmd} | conditional | flops 286661120 | bytes 19248296 | solution.py:113
  79.7 2.1 fusion.3
  81.9 1.5 fusion.10
  83.4 1.4 fusion.2
  89.5 3.3 %convolution_convert_fusion.1 = bf16[256,2048]{1,0:T(8,128)(2,1)} fusion(bf16[256,512]{0,1:T(8,128)(2,1)S(1)} %bitcast.88, bf16[512,2048]{1,0:T(8,128)(2,1)} %param.19), kind=kOutput, calls=%fused_computation.33 | convolution fusion | flops 537395200 | bytes 3407872 | tf_op jit(solution)/shard_map/dot_general | solution.py:136
  95.0 42.6 %reduce-scatter.3.cloned.1.call-done = bf16[64,2048]{1,0:T(8,128)(2,1)} async-done(((bf16[256,2048]{1,0:T(8,128)(2,1)}), bf16[64,2048]{1,0:T(8,128)(2,1)}) %reduce-scatter.3.cloned.1.call-update) | async-done | bytes 262160 | tf_op jit(solution)/shard_map/reduce_scatter | solution.py:135
  139.9 2.0 gather_fusion
  143.2 25.4 %all_to_all.10 = bf16[8,24,2048]{2,1,0:T(8,128)(2,1)} all-to-all(bf16[8,24,2048]{2,1,0:T(8,128)(2,1)S(1)} %broadcast_select_fusion), channel_id=1, replica_groups=mesh['sp'=8,'tp'=4] {'sp'}, dimensions={0} | all-to-all | bytes 1572864 | tf_op jit(solution)/shard_map/all_to_all | solution.py:155
  168.9 26.5 %all-gather.2.cloned.1.call-done = bf16[32,24,2048]{2,1,0:T(8,128)(2,1)} async-done(((bf16[8,24,2048]{2,1,0:T(8,128)(2,1)}), bf16[32,24,2048]{2,1,0:T(8,128)(2,1)}) %all-gather.2.cloned.1.call-update) | async-done | bytes 3145744 | tf_op jit(solution)/shard_map/all_gather | solution.py:156
  195.4 5.6 %fusion.19 = f32[768,768]{1,0:T(8,128)S(1)} fusion(bf16[768,2048]{1,0:T(8,128)(2,1)} %bitcast.91, bf16[1,2048,768]{2,1,0:T(8,128)(2,1)} %param.24), kind=kOutput, calls=%fused_computation.29 | convolution fusion | flops 2415919104 | bytes 8650752 | tf_op jit(solution)/shard_map/dot_general | solution.py:159
  201.0 2.9 multiply_convert_fusion
  203.9 4.0 %convolution_convert_fusion = bf16[32,24,2048]{2,1,0:T(8,128)(2,1)} fusion(bf16[32,24,768]{2,1,0:T(8,128)(2,1)S(1)} %bitcast.93, bf16[1,768,2048]{2,1,0:T(8,128)(2,1)S(1)} %copy-done), kind=kOutput, calls=%fused_computation.27 | convolution fusion | flops 2417491968 | bytes 7471104 | tf_op jit(solution)/shard_map/rcf,fd->rcd/dot_general | solution.py:167
  207.9 38.0 %reduce-scatter.5.cloned.1.call-done = bf16[8,24,2048]{2,1,0:T(8,128)(2,1)} async-done(((bf16[32,24,2048]{2,1,0:T(8,128)(2,1)}), bf16[8,24,2048]{2,1,0:T(8,128)(2,1)}) %reduce-scatter.5.cloned.1.call-update) | async-done | bytes 786448 | tf_op jit(solution)/shard_map/reduce_scatter | solution.py:166
  245.9 5.5 %all-to-all-start.1 = ((bf16[8,24,2048]{2,1,0:T(8,128)(2,1)}), bf16[8,24,2048]{2,1,0:T(8,128)(2,1)}, u32[]{:S(2)}, u32[]{:S(2)}) async-start(bf16[8,24,2048]{2,1,0:T(8,128)(2,1)} %reduce-scatter.5.cloned.1.call-done), calls=%async_computation.3 | async-start | bytes 1572864 | tf_op jit(solution)/shard_map/all_to_all | solution.py:174
  251.6 20.1 %all-to-all-done.1 = bf16[8,24,2048]{2,1,0:T(8,128)(2,1)} async-done(((bf16[8,24,2048]{2,1,0:T(8,128)(2,1)}), bf16[8,24,2048]{2,1,0:T(8,128)(2,1)}, u32[]{:S(2)}, u32[]{:S(2)}) %all-to-all-start.1) | async-done | bytes 786464 | tf_op jit(solution)/shard_map/all_to_all | solution.py:174
  271.6 3.5 %gather_fusion.1 = bf16[128,2048]{1,0:T(8,128)(2,1)} fusion(bf16[192,2048]{1,0:T(8,128)(2,1)} %bitcast.29, s32[1024]{0:T(1024)S(1)} %pad_clamp_fusion), kind=kCustom, calls=%fused_computation.1 | custom fusion | bytes 1049088 | tf_op jit(solution)/shard_map/gather | solution.py:175
  275.2 2.7 reshape.150
  277.8 2.8 multiply_reduce_fusion
  280.7 1.8 add_convert_fusion
  (67 shorter events, 11.3 us)
Async XLA Ops:
  6.5 197.3 %copy-start = (bf16[1,768,2048]{2,1,0:T(8,128)(2,1)S(1)}, bf16[1,768,2048]{2,1,0:T(8,128)(2,1)}, u32[]{:S(2)}) copy-start(bf16[1,768,2048]{2,1,0:T(8,128)(2,1)} %param.25) | copy-start | bytes 9437188
  6.5 131.1 %reduce-scatter.3.cloned.1.call-start = ((), (), s32[]{:S(2)}) async-start(), calls=%async_computation.4 | async-start | bytes 1310720 | tf_op jit(solution)/shard_map/reduce_scatter | solution.py:135
  79.7 2.2 copy-start.3
  83.4 1.4 copy-start.4
  88.4 4.5 %copy-start.6 = (s32[64,2]{0,1:T(2,128)S(1)}, s32[64,2]{0,1:T(2,128)}, u32[]{:S(2)}) copy-start(s32[64,2]{0,1:T(2,128)} %param.21) | copy-start | bytes 1540
  88.4 49.2 %copy-start.1 = (bf16[64,2048]{1,0:T(8,128)(2,1)S(1)}, bf16[64,2048]{1,0:T(8,128)(2,1)}, u32[]{:S(2)}) copy-start(bf16[64,2048]{1,0:T(8,128)(2,1)} %param.18) | copy-start | bytes 786436
  88.4 50.4 %copy-start.5 = (f32[2048]{0:T(1024)S(1)}, f32[2048]{0:T(1024)}, u32[]{:S(2)}) copy-start(f32[2048]{0:T(1024)} %param.20) | copy-start | bytes 24580
  92.9 102.5 %all-gather.2.cloned.1.call-start = ((), (), s32[]{:S(2)}) async-start(), calls=%async_computation.5 | async-start | bytes 3932160 | tf_op jit(solution)/shard_map/all_gather | solution.py:156
  168.6 77.3 %reduce-scatter.5.cloned.1.call-start = ((), (), s32[]{:S(2)}) async-start(), calls=%async_computation.6 | async-start | bytes 3932160 | tf_op jit(solution)/shard_map/reduce_scatter | solution.py:166
  195.4 5.6 %copy-start.8 = (bf16[1,2048,768]{2,1,0:T(8,128)(2,1)S(1)}, bf16[1,2048,768]{2,1,0:T(8,128)(2,1)}, u32[]{:S(2)}) copy-start(bf16[1,2048,768]{2,1,0:T(8,128)(2,1)} %param.23) | copy-start | bytes 9437188
  195.4 5.6 %copy-start.9 = (bf16[32,24,2048]{2,1,0:T(8,128)(2,1)S(1)}, bf16[32,24,2048]{2,1,0:T(8,128)(2,1)}, u32[]{:S(2)}) copy-start(bf16[32,24,2048]{2,1,0:T(8,128)(2,1)} %all-gather.2.cloned.1.call-done) | copy-start | bytes 9437188
  207.9 43.6 %copy-start.7 = (f32[64,2]{0,1:T(2,128)S(1)}, f32[64,2]{0,1:T(2,128)}, u32[]{:S(2)}) copy-start(f32[64,2]{0,1:T(2,128)} %param.22) | copy-start | bytes 1540
  245.9 25.7 %all-to-all-start.1 = ((bf16[8,24,2048]{2,1,0:T(8,128)(2,1)}), bf16[8,24,2048]{2,1,0:T(8,128)(2,1)}, u32[]{:S(2)}, u32[]{:S(2)}) async-start(bf16[8,24,2048]{2,1,0:T(8,128)(2,1)} %reduce-scatter.5.cloned.1.call-done), calls=%async_computation.3 | async-start | bytes 1572864 | tf_op jit(solution)/shard_map/all_to_all | solution.py:174
  271.6 9.0 %copy-start.2 = (bf16[64,2048]{1,0:T(8,128)(2,1)S(1)}, bf16[64,2048]{1,0:T(8,128)(2,1)}, u32[]{:S(2)}) copy-start(bf16[64,2048]{1,0:T(8,128)(2,1)} %param.18) | copy-start | bytes 786436
Sparse Core Ops, SparseCore 0:
  93.0 44.5 reduce-scatter.2
  168.8 26.5 all-gather.1
  208.0 37.8 reduce-scatter.4
where the time goes:
time: 290 us; the launch traced here: 289 us
  waiting for transfers between devices  127 us (44%)
  blocking collectives  91.7 us (32%)
  matrix products  19.4 us (7%)
  local copies, waits for them, and re-layouts  17.7 us (6%)
  between operations  13.3 us (5%)
  other arithmetic  11.2 us (4%)
  starting transfers between devices  5.78 us (2%)
    reduce_scatter x1, waiting for transfers between devices, local(): lax.psum_scatter(jnp.dot(row_block, out_weight, preferred_element_type=jn...  42.6 us
    reduce_scatter x1, waiting for transfers between devices, local(): lax.psum_scatter(jnp.einsum('rcf,fd->rcd', row_block, expert_down[0], pre...  38 us
    all_gather x1, blocking collectives, local(): kv_piece = lax.all_gather(key_value_pairs, 'sp', axis=0, tiled=True)  33.6 us
    all_gather x1, blocking collectives, local(): all_gates = lax.all_gather(forget_gate_total, 'sp', axis=0, tiled=True)  32.7 us
    all_gather x1, waiting for transfers between devices, local(): arrived = lax.all_gather(incoming, 'tp', axis=0, tiled=True)  26.5 us
    all_to_all x1, blocking collectives, local(): lax.all_to_all(outgoing, 'sp', split_axis=0, concat_axis=0, tiled=True)  25.4 us
    all_to_all x1, waiting for transfers between devices, local(): lax.all_to_all(summed, 'sp', split_axis=0, concat_axis=0, tiled=True)  20.1 us
  transfers between devices with their start and end apart: 4, of which 4 were waited for; matrix products, arithmetic and copies ran while one was open for 1% of the time, Pallas kernels for 0%

commit v1 on v0

v1 whole, which is shorter than its diff:
```python
import functools

import jax
import jax.numpy as jnp
from jax import lax
from jax.experimental import pallas as pl
from jax.experimental.pallas import tpu as pltpu
from jax.sharding import PartitionSpec as P

HEAD_SIZE = 64
NEG_FILL = -1e30
NORM_EPS = 1e-06
OUTER = 2
MESH = pl.DeviceIdType.MESH
F32 = jnp.float32
BF16 = jnp.bfloat16


def greet(peers_sp, sp_count, sp, tp, tp_peers):
    barrier = pltpu.get_barrier_semaphore()

    def signal(step, carry):
        pl.semaphore_signal(
            barrier, inc=1, device_id=(lax.rem(sp + step, sp_count), tp), device_id_type=MESH
        )
        return carry

    lax.fori_loop(1, sp_count, signal, 0)
    for peer in tp_peers:
        pl.semaphore_signal(barrier, inc=1, device_id=(sp, peer), device_id_type=MESH)
    return lambda: pl.semaphore_wait(barrier, sp_count - 1 + len(tp_peers))


def remote(src, dst, send, recv, device):
    return pltpu.make_async_remote_copy(
        src_ref=src,
        dst_ref=dst,
        send_sem=send,
        recv_sem=recv,
        device_id=device,
        device_id_type=MESH,
    )


def tp_places(tp, tp_count):
    inner = tp_count // OUTER
    a, c = tp // inner, lax.rem(tp, inner)
    mates = [a * inner + lax.rem(c + k, inner) for k in range(1, inner)]
    across = (1 - a) * inner + c
    return inner, a, c, mates, across


def mix_kernel(
    sp_count,
    tp_count,
    q_ref,
    kv_ref,
    gate_ref,
    gate_rows_ref,
    resid_ref,
    gain_ref,
    wout_hbm,
    hidden_ref,
    normed_ref,
    kv_all,
    gate_all,
    qm_ref,
    max_ref,
    acc_ref,
    att_ref,
    wout,
    mate_out,
    mate_in,
    own_sum,
    far_out,
    far_in,
    w_sem,
    kv_send,
    kv_recv,
    gate_send,
    gate_recv,
    mate_send,
    mate_recv,
    far_send,
    far_recv,
):
    sp, tp = lax.axis_index("sp"), lax.axis_index("tp")
    inner, a, c, mates, across = tp_places(tp, tp_count)
    rows, width = q_ref.shape
    heads = width // HEAD_SIZE
    pair = 2 * HEAD_SIZE
    groups = kv_ref.shape[1] // pair
    per_group = heads // groups
    own = rows // tp_count
    ready = greet(None, sp_count, sp, tp, mates + [across])
    load = pltpu.make_async_copy(wout_hbm, wout, w_sem)
    load.start()

    low = lax.broadcasted_iota(jnp.int32, (rows, pair), 1) < HEAD_SIZE
    for h in range(heads):
        base = (h // 2) * pair
        block = q_ref[:, base : base + pair].astype(F32) * (HEAD_SIZE**-0.5)
        keep = low if h % 2 == 0 else jnp.logical_not(low)
        qm_ref[h] = jnp.where(keep, block, 0.0).astype(BF16)
    ready()

    def kv_copy(source, target):
        return remote(
            kv_ref, kv_all.at[source], kv_send.at[target], kv_recv.at[source], (target, tp)
        )

    def gate_copy(source, target):
        return remote(
            gate_rows_ref,
            gate_all.at[source],
            gate_send.at[target],
            gate_recv.at[source],
            (target, tp),
        )

    def send(target, carry):
        kv_copy(sp, target).start()
        gate_copy(sp, target).start()
        return carry

    lax.fori_loop(sp + 1, sp_count, send, 0)

    def attend(kv, gates, first):
        causal = None
        if first:
            causal = lax.broadcasted_iota(jnp.int32, (rows, rows), 1) <= lax.broadcasted_iota(
                jnp.int32, (rows, rows), 0
            )
        for g in range(groups):
            both = kv[:, g * pair : (g + 1) * pair].astype(F32)
            swapped = pltpu.roll(both, HEAD_SIZE, 1)
            keys = jnp.where(low, both, swapped).astype(BF16)
            values = (
                jnp.where(low, swapped, 1.0).astype(BF16),
                jnp.where(low, 1.0, both).astype(BF16),
            )
            for h in range(g * per_group, (g + 1) * per_group):
                scores = lax.dot_general(
                    qm_ref[h], keys, (((1,), (1,)), ((), ())), preferred_element_type=F32
                )
                scores = scores + gate_ref[:, h : h + 1] - gates[h : h + 1, :]
                if first:
                    scores = jnp.where(causal, scores, NEG_FILL)
                top = jnp.max(scores, axis=1, keepdims=True)
                if not first:
                    old = max_ref[h]
                    top = jnp.maximum(old, top)
                weights = jnp.exp(scores - top).astype(BF16)
                block_sum = jnp.dot(weights, values[h % 2], preferred_element_type=F32)
                if first:
                    acc_ref[h] = block_sum
                else:
                    acc_ref[h] = acc_ref[h] * jnp.exp(old - top) + block_sum
                max_ref[h] = top

    attend(kv_ref[...], gate_rows_ref[...], True)

    def earlier(step, carry):
        source = sp - step
        kv_copy(source, sp).wait_recv()
        gate_copy(source, sp).wait_recv()
        attend(kv_all[source], gate_all[source], False)
        return carry

    lax.fori_loop(1, sp + 1, earlier, 0)

    for h in range(0, heads, 2):
        even, odd = acc_ref[h], acc_ref[h + 1]
        even = even / pltpu.roll(even, HEAD_SIZE, 1)
        odd = odd / pltpu.roll(odd, HEAD_SIZE, 1)
        att_ref[:, (h // 2) * pair : (h // 2 + 1) * pair] = jnp.where(low, even, odd).astype(BF16)

    load.wait()

    def product(column):
        parts = [
            att_ref[pl.ds(pl.multiple_of((o * inner + column) * own, own), own), :]
            for o in range(OUTER)
        ]
        return jnp.dot(jnp.concatenate(parts, axis=0), wout[...], preferred_element_type=F32)

    mate_copies = []
    for k, mate in enumerate(mates):
        mate_out[k] = product(lax.rem(mate, inner)).astype(BF16)
        copy = remote(
            mate_out.at[k], mate_in.at[k], mate_send.at[k], mate_recv.at[k], (sp, mate)
        )
        copy.start()
        mate_copies.append(copy)
    own_sum[...] = product(c).reshape(OUTER, own, own_sum.shape[2])
    for k, copy in enumerate(mate_copies):
        copy.wait_recv()
        own_sum[...] += mate_in[k].astype(F32).reshape(own_sum.shape)
    far_out[...] = own_sum[1 - a].astype(BF16)
    far = remote(far_out, far_in, far_send, far_recv, (sp, across))
    far.start()
    far.wait_recv()
    hidden = resid_ref[...].astype(F32) + own_sum[a] + far_in[...].astype(F32)
    hidden_ref[...] = hidden
    scale = lax.rsqrt(jnp.mean(hidden * hidden, axis=1, keepdims=True) + NORM_EPS)
    normed_ref[...] = (hidden * scale * gain_ref[...]).astype(BF16)
    far.wait_send()
    for copy in mate_copies:
        copy.wait_send()

    def finish(target, carry):
        kv_copy(sp, target).wait_send()
        gate_copy(sp, target).wait_send()
        return carry

    lax.fori_loop(sp + 1, sp_count, finish, 0)


def expert_kernel(
    sp_count,
    tp_count,
    cap,
    normed_ref,
    hidden_ref,
    slot_cols_ref,
    slot_rows_ref,
    weight_ref,
    gate_hbm,
    up_hbm,
    down_hbm,
    out_ref,
    outgoing,
    inbox,
    w_gate,
    w_up,
    w_down,
    partial,
    mate_in,
    chip_sum,
    far_in,
    final,
    back,
    w_sem,
    own_sem,
    s1,
    r1,
    s2,
    r2,
    s3,
    r3,
    s4,
    r4,
    s5,
    r5,
    s6,
    r6,
    s7,
    r7,
):
    sp, tp = lax.axis_index("sp"), lax.axis_index("tp")
    inner, a, c, mates, across = tp_places(tp, tp_count)
    own, width = normed_ref.shape
    slots = sp_count * cap
    ready = greet(None, sp_count, sp, tp, mates + [across])
    loads = [
        pltpu.make_async_copy(src.at[0], dst, w_sem.at[i])
        for i, (src, dst) in enumerate(
            ((gate_hbm, w_gate), (up_hbm, w_up), (down_hbm, w_down))
        )
    ]
    for load in loads:
        load.start()
    slot_at = lax.broadcasted_iota(jnp.int32, (slots, own), 0)
    chosen = slot_rows_ref[...]
    pick = jnp.zeros((slots, own), F32)
    for k in range(chosen.shape[0]):
        pick = pick + jnp.where(slot_at == chosen[k : k + 1, :], 1.0, 0.0)
    sent = jnp.dot(pick.astype(BF16), normed_ref[...], preferred_element_type=F32)
    outgoing[...] = sent.reshape(sp_count, cap, width).astype(BF16)
    ready()

    def at(step):
        return lax.rem(sp + step, sp_count)

    def before(step):
        return lax.rem(sp + sp_count - step, sp_count)

    def to_expert(target, source):
        return remote(
            outgoing.at[target], inbox.at[source, c, a], s1.at[target], r1.at[source], (target, tp)
        )

    def to_across(source):
        return remote(
            inbox.at[source, c, a], inbox.at[source, c, a], s2.at[source], r2.at[source], (sp, across)
        )

    def from_across(source):
        return remote(
            inbox.at[source, c, a],
            inbox.at[source, c, 1 - a],
            s2.at[source],
            r2.at[source],
            (sp, across),
        )

    def to_mate(k, source, o, send, recv):
        return remote(
            inbox.at[source, c, o], inbox.at[source, c, o], send.at[k, source], recv.at[k, source],
            (sp, mates[k]),
        )

    def from_mate(k, source, o, send, recv):
        sender = lax.rem(c + inner - (k + 1), inner)
        return remote(
            inbox.at[source, c, o],
            inbox.at[source, sender, o],
            send.at[k, source],
            recv.at[k, source],
            (sp, mates[k]),
        )

    def start_one(step, carry):
        to_expert(at(step), sp).start()
        return carry

    lax.fori_loop(1, sp_count, start_one, 0)
    keep = pltpu.make_async_copy(outgoing.at[sp], inbox.at[sp, c, a], own_sem)
    keep.start()
    keep.wait()

    def forward(source):
        to_across(source).start()
        for k in range(len(mates)):
            to_mate(k, source, a, s3, r3).start()

    def forward_across(source):
        from_across(source).wait_recv()
        for k in range(len(mates)):
            to_mate(k, source, 1 - a, s4, r4).start()

    forward(sp)

    def dispatch(step, carry):
        source = before(step)
        to_expert(sp, source).wait_recv()
        forward(source)
        forward_across(before(step - 1))
        return carry

    lax.fori_loop(1, sp_count, dispatch, 0)
    forward_across(before(sp_count - 1))
    for load in loads:
        load.wait()

    def compute(step):
        source = before(step)
        for k in range(len(mates)):
            from_mate(k, source, a, s3, r3).wait_recv()
            from_mate(k, source, 1 - a, s4, r4).wait_recv()

    def load_rows(source):
        return inbox[source].astype(F32).reshape(tp_count * cap, width).astype(BF16)

    def send_mate(k, source):
        return remote(
            partial.at[source, lax.rem(mates[k], inner)],
            mate_in.at[k, source],
            s5.at[k, source],
            r5.at[k, source],
            (sp, mates[k]),
        )

    def send_far(source):
        return remote(
            chip_sum.at[source, 1 - a], far_in.at[source], s6.at[source], r6.at[source], (sp, across)
        )

    def send_back(target, source):
        return remote(
            final.at[target], back.at[source], s7.at[target], r7.at[source], (target, tp)
        )

    batch = 2 if sp_count % 2 == 0 else 1
    steps = sp_count // batch

    def ffn(i):
        for b in range(batch):
            compute(i * batch + b)
        x = jnp.concatenate([load_rows(before(i * batch + b)) for b in range(batch)], axis=0)
        gate = jnp.dot(x, w_gate[...], preferred_element_type=F32)
        up = jnp.dot(x, w_up[...], preferred_element_type=F32)
        hidden = (gate / (1.0 + jnp.exp(-gate)) * up).astype(BF16)
        y = jnp.dot(hidden, w_down[...], preferred_element_type=F32)
        y = y.reshape(batch, inner, OUTER, cap, width).astype(BF16)
        for b in range(batch):
            source = before(i * batch + b)
            partial[source] = y[b]
            for k in range(len(mates)):
                send_mate(k, source).start()

    def chip(i):
        for b in range(batch):
            source = before(i * batch + b)
            total = partial[source, c].astype(F32)
            for k in range(len(mates)):
                send_mate(k, source).wait_recv()
                total = total + mate_in[k, source].astype(F32)
            chip_sum[source] = total.astype(BF16)
            send_far(source).start()

    def give_back(i):
        for b in range(batch):
            step = i * batch + b
            source = before(step)
            send_far(source).wait_recv()
            total = chip_sum[source, a].astype(F32) + far_in[source].astype(F32)
            final[source] = total.astype(BF16)

            @pl.when(step > 0)
            def _():
                send_back(source, sp).start()

    def pipeline(i, carry):
        ffn(i)

        @pl.when(i >= 1)
        def _():
            chip(i - 1)

        @pl.when(i >= 2)
        def _():
            give_back(i - 2)

        return carry

    lax.fori_loop(0, steps, pipeline, 0)
    chip(steps - 1)
    if steps >= 2:
        give_back(steps - 2)
    give_back(steps - 1)
    back[sp] = final[sp]

    slot_of = lax.broadcasted_iota(jnp.int32, (own, slots), 1)
    share = jnp.zeros((own, slots), F32)
    for k in range(slot_cols_ref.shape[1]):
        share = share + jnp.where(
            slot_of == slot_cols_ref[:, k : k + 1], weight_ref[:, k : k + 1], 0.0
        )
    high = share.astype(BF16)
    rest = share - high.astype(F32)
    middle = rest.astype(BF16)
    least = (rest - middle.astype(F32)).astype(BF16)

    def arrive(step, carry):
        send_back(sp, at(step)).wait_recv()
        return carry

    lax.fori_loop(1, sp_count, arrive, 0)
    results = back[...].astype(F32).reshape(slots, width).astype(BF16)
    combined = hidden_ref[...]
    for piece in (high, middle, least):
        combined = combined + jnp.dot(piece, results, preferred_element_type=F32)
    out_ref[...] = combined.astype(BF16)

    def finish(step, carry):
        source = at(step)
        to_across(source).wait_send()
        send_far(source).wait_send()
        for k in range(len(mates)):
            to_mate(k, source, a, s3, r3).wait_send()
            to_mate(k, source, 1 - a, s4, r4).wait_send()
            send_mate(k, source).wait_send()

        @pl.when(step > 0)
        def _():
            to_expert(source, sp).wait_send()
            send_back(source, sp).wait_send()

        return carry

    lax.fori_loop(0, sp_count, finish, 0)


def local(
    queries,
    key_value_pairs,
    forget_gate_total,
    residual_in,
    out_weight,
    norm_gain,
    routes,
    route_weight,
    expert_gate,
    expert_up,
    expert_down,
):
    sp_count = lax.axis_size("sp")
    tp_count = lax.axis_size("tp")
    rows, q_width = queries.shape
    heads = q_width // HEAD_SIZE
    own, width = residual_in.shape
    inner = tp_count // OUTER
    vmem = pl.BlockSpec(memory_space=pltpu.VMEM)
    hbm = pl.BlockSpec(memory_space=pl.ANY)
    dma = pltpu.SemaphoreType.DMA
    hidden, normed = pl.pallas_call(
        functools.partial(mix_kernel, sp_count, tp_count),
        out_shape=(
            jax.ShapeDtypeStruct((own, width), F32),
            jax.ShapeDtypeStruct((own, width), BF16),
        ),
        in_specs=[vmem] * 6 + [hbm],
        out_specs=(vmem, vmem),
        scratch_shapes=[
            pltpu.VMEM((sp_count, rows, key_value_pairs.shape[1]), BF16),
            pltpu.VMEM((sp_count, heads, rows), F32),
            pltpu.VMEM((heads, rows, 2 * HEAD_SIZE), BF16),
            pltpu.VMEM((heads, rows, 1), F32),
            pltpu.VMEM((heads, rows, 2 * HEAD_SIZE), F32),
            pltpu.VMEM((rows, q_width), BF16),
            pltpu.VMEM(out_weight.shape, BF16),
            pltpu.VMEM((inner - 1, OUTER * own, width), BF16),
            pltpu.VMEM((inner - 1, OUTER * own, width), BF16),
            pltpu.VMEM((OUTER, own, width), F32),
            pltpu.VMEM((own, width), BF16),
            pltpu.VMEM((own, width), BF16),
            dma,
            dma((sp_count,)),
            dma((sp_count,)),
            dma((sp_count,)),
            dma((sp_count,)),
            dma((inner - 1,)),
            dma((inner - 1,)),
            dma,
            dma,
        ],
        compiler_params=pltpu.CompilerParams(
            collective_id=0, has_side_effects=True, vmem_limit_bytes=40 * 2**20
        ),
        name="mix",
    )(
        queries,
        key_value_pairs,
        forget_gate_total,
        forget_gate_total.T,
        residual_in,
        norm_gain.reshape(1, -1),
        out_weight,
    )

    top = routes.shape[1]
    cap = max(2, 3 * own * top // (2 * sp_count))
    cap = -(-cap // 8) * 8
    flat = routes.reshape(-1)
    order = jnp.arange(flat.shape[0], dtype=jnp.int32)
    same = (flat[:, None] == flat[None, :]) & (order[None, :] < order[:, None])
    slot = (flat * cap + jnp.sum(same.astype(jnp.int32), axis=1)).reshape(own, top)
    ff = expert_gate.shape[2]
    block = (cap, width)
    return pl.pallas_call(
        functools.partial(expert_kernel, sp_count, tp_count, cap),
        out_shape=jax.ShapeDtypeStruct((own, width), BF16),
        in_specs=[vmem] * 5 + [hbm] * 3,
        out_specs=vmem,
        scratch_shapes=[
            pltpu.VMEM((sp_count,) + block, BF16),
            pltpu.VMEM((sp_count, inner, OUTER) + block, BF16),
            pltpu.VMEM((width, ff), BF16),
            pltpu.VMEM((width, ff), BF16),
            pltpu.VMEM((ff, width), BF16),
            pltpu.VMEM((sp_count, inner, OUTER) + block, BF16),
            pltpu.VMEM((inner - 1, sp_count, OUTER) + block, BF16),
            pltpu.VMEM((sp_count, OUTER) + block, BF16),
            pltpu.VMEM((sp_count,) + block, BF16),
            pltpu.VMEM((sp_count,) + block, BF16),
            pltpu.VMEM((sp_count,) + block, BF16),
            dma((3,)),
            dma,
            dma((sp_count,)),
            dma((sp_count,)),
            dma((sp_count,)),
            dma((sp_count,)),
            dma((inner - 1, sp_count)),
            dma((inner - 1, sp_count)),
            dma((inner - 1, sp_count)),
            dma((inner - 1, sp_count)),
            dma((inner - 1, sp_count)),
            dma((inner - 1, sp_count)),
            dma((sp_count,)),
            dma((sp_count,)),
            dma((sp_count,)),
            dma((sp_count,)),
        ],
        compiler_params=pltpu.CompilerParams(
            collective_id=1, has_side_effects=True, vmem_limit_bytes=60 * 2**20
        ),
        name="experts",
    )(normed, hidden, slot, slot.T, route_weight, expert_gate, expert_up, expert_down)


def solution(mesh):
    return jax.shard_map(
        local,
        mesh=mesh,
        in_specs=(
            P("sp", "tp"),
            P("sp", "tp"),
            P("sp", "tp"),
            P(("sp", "tp"), None),
            P("tp", None),
            P(),
            P(("sp", "tp"), None),
            P(("sp", "tp"), None),
            P("sp", None, "tp"),
            P("sp", None, "tp"),
            P("sp", "tp", None),
        ),
        out_specs=P(("sp", "tp"), None),
        check_vma=False,
    )
```

time: 290 us -> 117 us (0.40)
  waiting for transfers between devices: 127 us -> 0 us
  Pallas kernels: 0 us -> 103 us
  blocking collectives: 91.7 us -> 0 us
  matrix products: 19.4 us -> 0 us
  between operations: 13.3 us -> 0.07 us
  other arithmetic: 11.2 us -> 0.88 us
  starting transfers between devices: 5.78 us -> 0 us
  local copies, waits for them, and re-layouts: 17.7 us -> 12.9 us
    pallas_call x0 -> x2, Pallas kernels: none -> 103 us  [the longest x1 84.1 us: local(): pl.pallas_call(functools.partial(expert_kernel, sp_count, tp_count, cap),...]
    reduce_scatter x2 -> x0, waiting for transfers between devices: 80.7 us -> none  [the longest x1 42.6 us: local(): lax.psum_scatter(jnp.dot(row_block, out_weight, preferred_element_type=jn...]
    all_gather x2 -> x0, blocking collectives: 66.2 us -> none  [the longest x1 33.6 us: local(): kv_piece = lax.all_gather(key_value_pairs, 'sp', axis=0, tiled=True)]
    all_gather x1 -> x0, waiting for transfers between devices: 26.5 us -> none  [local(): arrived = lax.all_gather(incoming, 'tp', axis=0, tiled=True)]
    all_to_all x1 -> x0, blocking collectives: 25.4 us -> none  [local(): lax.all_to_all(outgoing, 'sp', split_axis=0, concat_axis=0, tiled=True)]
    all_to_all x1 -> x0, waiting for transfers between devices: 20.1 us -> none  [local(): lax.all_to_all(summed, 'sp', split_axis=0, concat_axis=0, tiled=True)]
    dot_general x6 -> x0, matrix products: 19.4 us -> none  [the longest x1 5.58 us: local(): jnp.dot(flat_in, expert_up[0], preferred_element_type=jnp.float32)]
    unnamed x19 -> x22, local copies, waits for them, and re-layouts: 2.02 us -> 11.8 us
  transfers between devices with their start and end apart: 4 -> 0, of which waited for: 4 -> 0; matrix products, arithmetic and copies ran while one was open for 1% -> 0% of each run, Pallas kernels for 0% -> 0%
where the time goes in v1:
time: 117 us
  Pallas kernels  103 us (88%)
  local copies, waits for them, and re-layouts  12.9 us (11%)
    pallas_call x1, Pallas kernels, local(): pl.pallas_call(functools.partial(expert_kernel, sp_count, tp_count, cap),...  84.1 us
    pallas_call x1, Pallas kernels, local(): pl.pallas_call(functools.partial(mix_kernel, sp_count, tp_count), out_sha...  18.7 us
    unnamed x22, local copies, waits for them, and re-layouts  11.8 us

profile of v1, /device:TPU:0, one launch (start us, length us, event | category | flops | bytes accessed | tf_op | source)
XLA Modules:
  0.0 116.5 jit_solution(11271200155024475032)
XLA Ops:
  0.0 1.4 %copy.26.weight_ref = f32[64,2]{1,0:T(8,128)} copy(f32[64,2]{0,1:T(2,128)} %param.18) | data formatting | bytes 1024 | tf_op args[7]
  1.4 0.8 copy.23
  2.1 0.1 eq.15
  2.3 0.2 convert_reduce_fusion
  2.5 0.1 reduce_sum.12
  2.6 0.1 copy.24
  2.7 0.7 multiply_add_fusion
  3.4 0.0 copy-start.8
  3.4 0.7 copy.25.slot_cols_ref
  4.1 0.8 copy.22.gate_ref
  4.9 0.0 copy-start
  4.9 1.6 %copy-done = bf16[512,2048]{1,0:T(8,128)(2,1)S(1)} copy-done((bf16[512,2048]{1,0:T(8,128)(2,1)S(1)}, bf16[512,2048]{1,0:T(8,128)(2,1)}, u32[]{:S(2)}) %copy-start) | copy-done | bytes 2097176
  6.5 0.9 copy-done.3
  7.4 0.9 copy-done.4
  8.4 0.8 copy-done.5
  9.2 0.7 copy-done.6
  9.9 0.7 copy-done.7
  10.6 18.7 %mix.1 = (f32[64,2048]{1,0:T(8,128)S(1)}, bf16[64,2048]{1,0:T(8,128)(2,1)S(1)}) custom-call(bf16[256,512]{1,0:T(8,128)(2,1)S(1)} %copy-done.3, bf16[256,128]{1,0:T(8,128)(2,1)S(1)} %copy-done.5, f32[256,8]{1,0:T(8,128)S(1)} %copy.22.gate_ref, f32[8,256]{1,0:T(8,128)S(1)} %bitcast.3, bf16[64,2048]{1,0:T(8,128)(2,1)S(1)} %copy-done.4, f32[1,2048]{1,0:T(1,128)S(1)} %bitcast.4, ...), custom_call_target="tpu_custom_call" | custom-call | tf_op jit(solution)/shard_map/mix/pallas_call | solution.py:507
  29.3 0.0 copy-start.1
  29.3 0.8 copy-done.1
  30.1 0.7 copy-done.2
  30.8 0.0 copy-done.8
  30.8 84.1 %experts.1 = bf16[64,2048]{1,0:T(8,128)(2,1)} custom-call(bf16[64,2048]{1,0:T(8,128)(2,1)} %copy-done.2, f32[64,2048]{1,0:T(8,128)} %copy-done.1, s32[64,2]{1,0:T(8,128)} %copy.25.slot_cols_ref, s32[2,64]{1,0:T(2,128)} %bitcast.5, f32[64,2]{1,0:T(8,128)} %copy.26.weight_ref, bf16[1,2048,768]{2,1,0:T(8,128)(2,1)} %gate_hbm.1, bf16[1,2048,768]{2,1,0:T(8,128)(2,1)} %up_hbm.1, ...), custom_call_target="tpu_custom_call" | custom-call | tf_op jit(solution)/shard_map/experts/pallas_call | solution.py:561
  114.9 1.7 %copy.28 = bf16[64,2048]{1,0:T(8,128)(2,1)} copy(bf16[64,2048]{1,0:T(8,128)(2,1)} %experts.1) | data formatting | bytes 524288
  (6 shorter events, 0.0 us)
Async XLA Ops:
  3.4 27.4 %copy-start.8 = (s32[64,2]{0,1:T(2,128)}, s32[64,2]{0,1:T(2,128)S(1)}, u32[]{:S(2)}) copy-start(s32[64,2]{0,1:T(2,128)S(1)} %multiply_add_fusion) | copy-start | bytes 1540
  4.9 1.6 %copy-start = (bf16[512,2048]{1,0:T(8,128)(2,1)S(1)}, bf16[512,2048]{1,0:T(8,128)(2,1)}, u32[]{:S(2)}) copy-start(bf16[512,2048]{1,0:T(8,128)(2,1)} %wout_hbm.1) | copy-start | bytes 6291460
  6.5 0.9 copy-start.3
  7.4 0.9 copy-start.4
  8.4 0.8 copy-start.5
  9.2 0.7 copy-start.6
  9.9 0.7 copy-start.7
  29.3 0.8 copy-start.1
  30.1 0.7 copy-start.2

commit v2 on v1

--- a/solution.py
+++ b/solution.py
@@ -50,30 +50,55 @@
     return inner, a, c, mates, across
 
 
-def mix_kernel(
+def layer_kernel(
     sp_count,
     tp_count,
+    cap,
+    q_hbm,
+    kv_hbm,
+    gates_hbm,
+    resid_hbm,
+    gain_hbm,
+    wout_hbm,
+    routes_hbm,
+    weight_hbm,
+    gate_hbm,
+    up_hbm,
+    down_hbm,
+    out_ref,
     q_ref,
     kv_ref,
-    gate_ref,
     gate_rows_ref,
     resid_ref,
     gain_ref,
-    wout_hbm,
-    hidden_ref,
-    normed_ref,
+    routes_ref,
+    weight_ref,
     kv_all,
     gate_all,
+    gate_ref,
     qm_ref,
     max_ref,
     acc_ref,
     att_ref,
     wout,
     mate_out,
-    mate_in,
+    mate_back,
     own_sum,
     far_out,
+    far_back,
+    hidden_ref,
+    outgoing,
+    inbox,
+    w_gate,
+    w_up,
+    w_down,
+    partial,
+    mate_in,
+    chip_sum,
     far_in,
+    final,
+    back,
+    in_sem,
     w_sem,
     kv_send,
     kv_recv,
@@ -83,47 +108,90 @@
     mate_recv,
     far_send,
     far_recv,
+    own_sem,
+    s1,
+    r1,
+    s2,
+    r2,
+    s3,
+    r3,
+    s4,
+    r4,
+    s5,
+    r5,
+    s6,
+    r6,
+    s7,
+    r7,
 ):
     sp, tp = lax.axis_index("sp"), lax.axis_index("tp")
     inner, a, c, mates, across = tp_places(tp, tp_count)
-    rows, width = q_ref.shape
-    heads = width // HEAD_SIZE
+    rows, q_width = q_ref.shape
+    heads = q_width // HEAD_SIZE
     pair = 2 * HEAD_SIZE
     groups = kv_ref.shape[1] // pair
     per_group = heads // groups
     own = rows // tp_count
     ready = greet(None, sp_count, sp, tp, mates + [across])
-    load = pltpu.make_async_copy(wout_hbm, wout, w_sem)
-    load.start()
-
+    fetches = [
+        pltpu.make_async_copy(src, dst, in_sem.at[i])
+        for i, (src, dst) in enumerate(
+            (
+                (kv_hbm, kv_ref),
+                (gates_hbm, gate_rows_ref),
+                (q_hbm, q_ref),
+                (routes_hbm, routes_ref),
+                (weight_hbm, weight_ref),
+                (resid_hbm, resid_ref),
+                (gain_hbm, gain_ref),
+                (wout_hbm, wout),
+            )
+        )
+    ]
+    for fetch in fetches:
+        fetch.start()
+    loads = [
+        pltpu.make_async_copy(src.at[0], dst, w_sem.at[i])
+        for i, (src, dst) in enumerate(
+            ((gate_hbm, w_gate), (up_hbm, w_up), (down_hbm, w_down))
+        )
+    ]
+    for load in loads:
+        load.start()
+    fetches[0].wait()
+    fetches[1].wait()
+    ready()
+
+
+    def kv_copy(source, target):
+        return remote(
+            kv_ref, kv_all.at[source], kv_send.at[target], kv_recv.at[source], (target, tp)
+        )
+
+    def gate_copy(source, target):
+        return remote(
+            gate_rows_ref,
+            gate_all.at[source],
+            gate_send.at[target],
+            gate_recv.at[source],
+            (target, tp),
+        )
+
+    def send(target, carry):
+        kv_copy(sp, target).start()
+        gate_copy(sp, target).start()
+        return carry
+
+    lax.fori_loop(sp + 1, sp_count, send, 0)
+
+    fetches[2].wait()
+    gate_ref[...] = gate_rows_ref[...].T
     low = lax.broadcasted_iota(jnp.int32, (rows, pair), 1) < HEAD_SIZE
     for h in range(heads):
         base = (h // 2) * pair
         block = q_ref[:, base : base + pair].astype(F32) * (HEAD_SIZE**-0.5)
         keep = low if h % 2 == 0 else jnp.logical_not(low)
         qm_ref[h] = jnp.where(keep, block, 0.0).astype(BF16)
-    ready()
-
-    def kv_copy(source, target):
-        return remote(
-            kv_ref, kv_all.at[source], kv_send.at[target], kv_recv.at[source], (target, tp)
-        )
-
-    def gate_copy(source, target):
-        return remote(
-            gate_rows_ref,
-            gate_all.at[source],
-            gate_send.at[target],
-            gate_recv.at[source],
-            (target, tp),
-        )
-
-    def send(target, carry):
-        kv_copy(sp, target).start()
-        gate_copy(sp, target).start()
-        return carry
-
-    lax.fori_loop(sp + 1, sp_count, send, 0)
 
     def attend(kv, gates, first):
         causal = None
@@ -175,7 +243,8 @@
         odd = odd / pltpu.roll(odd, HEAD_SIZE, 1)
         att_ref[:, (h // 2) * pair : (h // 2 + 1) * pair] = jnp.where(low, even, odd).astype(BF16)
 
-    load.wait()
+    for fetch in fetches[3:]:
+        fetch.wait()
 
     def product(column):
         parts = [
@@ -188,96 +257,46 @@
     for k, mate in enumerate(mates):
         mate_out[k] = product(lax.rem(mate, inner)).astype(BF16)
         copy = remote(
-            mate_out.at[k], mate_in.at[k], mate_send.at[k], mate_recv.at[k], (sp, mate)
+            mate_out.at[k], mate_back.at[k], mate_send.at[k], mate_recv.at[k], (sp, mate)
         )
         copy.start()
         mate_copies.append(copy)
     own_sum[...] = product(c).reshape(OUTER, own, own_sum.shape[2])
     for k, copy in enumerate(mate_copies):
         copy.wait_recv()
-        own_sum[...] += mate_in[k].astype(F32).reshape(own_sum.shape)
+        own_sum[...] += mate_back[k].astype(F32).reshape(own_sum.shape)
     far_out[...] = own_sum[1 - a].astype(BF16)
-    far = remote(far_out, far_in, far_send, far_recv, (sp, across))
+    far = remote(far_out, far_back, far_send, far_recv, (sp, across))
     far.start()
     far.wait_recv()
-    hidden = resid_ref[...].astype(F32) + own_sum[a] + far_in[...].astype(F32)
+    hidden = resid_ref[...].astype(F32) + own_sum[a] + far_back[...].astype(F32)
     hidden_ref[...] = hidden
     scale = lax.rsqrt(jnp.mean(hidden * hidden, axis=1, keepdims=True) + NORM_EPS)
-    normed_ref[...] = (hidden * scale * gain_ref[...]).astype(BF16)
-    far.wait_send()
-    for copy in mate_copies:
-        copy.wait_send()
-
-    def finish(target, carry):
-        kv_copy(sp, target).wait_send()
-        gate_copy(sp, target).wait_send()
-        return carry
-
-    lax.fori_loop(sp + 1, sp_count, finish, 0)
-
-
-def expert_kernel(
-    sp_count,
-    tp_count,
-    cap,
-    normed_ref,
-    hidden_ref,
-    slot_cols_ref,
-    slot_rows_ref,
-    weight_ref,
-    gate_hbm,
-    up_hbm,
-    down_hbm,
-    out_ref,
-    outgoing,
-    inbox,
-    w_gate,
-    w_up,
-    w_down,
-    partial,
-    mate_in,
-    chip_sum,
-    far_in,
-    final,
-    back,
-    w_sem,
-    own_sem,
-    s1,
-    r1,
-    s2,
-    r2,
-    s3,
-    r3,
-    s4,
-    r4,
-    s5,
-    r5,
-    s6,
-    r6,
-    s7,
-    r7,
-):
-    sp, tp = lax.axis_index("sp"), lax.axis_index("tp")
-    inner, a, c, mates, across = tp_places(tp, tp_count)
-    own, width = normed_ref.shape
+    normed = (hidden * scale * gain_ref[...]).astype(BF16)
+
+    width = out_ref.shape[1]
     slots = sp_count * cap
-    ready = greet(None, sp_count, sp, tp, mates + [across])
-    loads = [
-        pltpu.make_async_copy(src.at[0], dst, w_sem.at[i])
-        for i, (src, dst) in enumerate(
-            ((gate_hbm, w_gate), (up_hbm, w_up), (down_hbm, w_down))
-        )
-    ]
-    for load in loads:
-        load.start()
-    slot_at = lax.broadcasted_iota(jnp.int32, (slots, own), 0)
-    chosen = slot_rows_ref[...]
+    top_count = routes_ref.shape[0]
+    expert_at = lax.broadcasted_iota(jnp.int32, (sp_count, own), 0)
+    earlier_row = lax.broadcasted_iota(jnp.int32, (own, own), 0) < lax.broadcasted_iota(
+        jnp.int32, (own, own), 1
+    )
+    ahead = jnp.where(earlier_row, 1.0, 0.0).astype(BF16)
+    slot_at = lax.broadcasted_iota(jnp.int32, (slots, own), 0).astype(F32)
+    first_slot = expert_at.astype(F32) * cap
+    taken = jnp.zeros((sp_count, 1), F32)
     pick = jnp.zeros((slots, own), F32)
-    for k in range(chosen.shape[0]):
-        pick = pick + jnp.where(slot_at == chosen[k : k + 1, :], 1.0, 0.0)
-    sent = jnp.dot(pick.astype(BF16), normed_ref[...], preferred_element_type=F32)
+    share = jnp.zeros((slots, own), F32)
+    for k in range(top_count):
+        named = jnp.where(expert_at == routes_ref[k : k + 1, :], 1.0, 0.0)
+        rank = jnp.dot(named.astype(BF16), ahead, preferred_element_type=F32)
+        slot = jnp.sum(named * (first_slot + rank + taken), axis=0, keepdims=True)
+        taken = taken + jnp.sum(named, axis=1, keepdims=True)
+        hit = slot_at == slot
+        pick = pick + jnp.where(hit, 1.0, 0.0)
+        share = share + jnp.where(hit, weight_ref[k : k + 1, :], 0.0)
+    sent = jnp.dot(pick.astype(BF16), normed, preferred_element_type=F32)
     outgoing[...] = sent.reshape(sp_count, cap, width).astype(BF16)
-    ready()
 
     def at(step):
         return lax.rem(sp + step, sp_count)
@@ -321,7 +340,7 @@
         )
 
     def start_one(step, carry):
-        to_expert(at(step), sp).start()
+        to_expert(before(step), sp).start()
         return carry
 
     lax.fori_loop(1, sp_count, start_one, 0)
@@ -339,22 +358,17 @@
         for k in range(len(mates)):
             to_mate(k, source, 1 - a, s4, r4).start()
 
-    forward(sp)
-
-    def dispatch(step, carry):
-        source = before(step)
-        to_expert(sp, source).wait_recv()
+    def accept(step):
+        source = at(step)
+
+        @pl.when(step > 0)
+        def _():
+            to_expert(sp, source).wait_recv()
+
         forward(source)
-        forward_across(before(step - 1))
-        return carry
-
-    lax.fori_loop(1, sp_count, dispatch, 0)
-    forward_across(before(sp_count - 1))
-    for load in loads:
-        load.wait()
-
-    def compute(step):
-        source = before(step)
+
+    def arrived(step):
+        source = at(step)
         for k in range(len(mates)):
             from_mate(k, source, a, s3, r3).wait_recv()
             from_mate(k, source, 1 - a, s4, r4).wait_recv()
@@ -386,22 +400,22 @@
 
     def ffn(i):
         for b in range(batch):
-            compute(i * batch + b)
-        x = jnp.concatenate([load_rows(before(i * batch + b)) for b in range(batch)], axis=0)
+            arrived(i * batch + b)
+        x = jnp.concatenate([load_rows(at(i * batch + b)) for b in range(batch)], axis=0)
         gate = jnp.dot(x, w_gate[...], preferred_element_type=F32)
         up = jnp.dot(x, w_up[...], preferred_element_type=F32)
         hidden = (gate / (1.0 + jnp.exp(-gate)) * up).astype(BF16)
         y = jnp.dot(hidden, w_down[...], preferred_element_type=F32)
         y = y.reshape(batch, inner, OUTER, cap, width).astype(BF16)
         for b in range(batch):
-            source = before(i * batch + b)
+            source = at(i * batch + b)
             partial[source] = y[b]
             for k in range(len(mates)):
                 send_mate(k, source).start()
 
     def chip(i):
         for b in range(batch):
-            source = before(i * batch + b)
+            source = at(i * batch + b)
             total = partial[source, c].astype(F32)
             for k in range(len(mates)):
                 send_mate(k, source).wait_recv()
@@ -412,7 +426,7 @@
     def give_back(i):
         for b in range(batch):
             step = i * batch + b
-            source = before(step)
+            source = at(step)
             send_far(source).wait_recv()
             total = chip_sum[source, a].astype(F32) + far_in[source].astype(F32)
             final[source] = total.astype(BF16)
@@ -422,6 +436,13 @@
                 send_back(source, sp).start()
 
     def pipeline(i, carry):
+        @pl.when(i + 1 < steps)
+        def _():
+            for b in range(batch):
+                accept((i + 1) * batch + b)
+
+        for b in range(batch):
+            forward_across(at(i * batch + b))
         ffn(i)
 
         @pl.when(i >= 1)
@@ -434,6 +455,10 @@
 
         return carry
 
+    for b in range(batch):
+        accept(b)
+    for load in loads:
+        load.wait()
     lax.fori_loop(0, steps, pipeline, 0)
     chip(steps - 1)
     if steps >= 2:
@@ -441,12 +466,6 @@
     give_back(steps - 1)
     back[sp] = final[sp]
 
-    slot_of = lax.broadcasted_iota(jnp.int32, (own, slots), 1)
-    share = jnp.zeros((own, slots), F32)
-    for k in range(slot_cols_ref.shape[1]):
-        share = share + jnp.where(
-            slot_of == slot_cols_ref[:, k : k + 1], weight_ref[:, k : k + 1], 0.0
-        )
     high = share.astype(BF16)
     rest = share - high.astype(F32)
     middle = rest.astype(BF16)
@@ -460,7 +479,9 @@
     results = back[...].astype(F32).reshape(slots, width).astype(BF16)
     combined = hidden_ref[...]
     for piece in (high, middle, least):
-        combined = combined + jnp.dot(piece, results, preferred_element_type=F32)
+        combined = combined + lax.dot_general(
+            piece, results, (((0,), (0,)), ((), ())), preferred_element_type=F32
+        )
     out_ref[...] = combined.astype(BF16)
 
     def finish(step, carry):
@@ -480,6 +501,16 @@
         return carry
 
     lax.fori_loop(0, sp_count, finish, 0)
+    far.wait_send()
+    for copy in mate_copies:
+        copy.wait_send()
+
+    def finish_mix(target, carry):
+        kv_copy(sp, target).wait_send()
+        gate_copy(sp, target).wait_send()
+        return carry
+
+    lax.fori_loop(sp + 1, sp_count, finish_mix, 0)
 
 
 def local(
@@ -501,20 +532,30 @@
     heads = q_width // HEAD_SIZE
     own, width = residual_in.shape
     inner = tp_count // OUTER
-    vmem = pl.BlockSpec(memory_space=pltpu.VMEM)
+    top = routes.shape[1]
+    cap = max(2, 3 * own * top // (2 * sp_count))
+    cap = -(-cap // 8) * 8
+    ff = expert_gate.shape[2]
+    block = (cap, width)
+    dma = pltpu.SemaphoreType.DMA
+    some, mate = dma((sp_count,)), dma((inner - 1, sp_count))
     hbm = pl.BlockSpec(memory_space=pl.ANY)
-    dma = pltpu.SemaphoreType.DMA
-    hidden, normed = pl.pallas_call(
-        functools.partial(mix_kernel, sp_count, tp_count),
-        out_shape=(
-            jax.ShapeDtypeStruct((own, width), F32),
-            jax.ShapeDtypeStruct((own, width), BF16),
-        ),
-        in_specs=[vmem] * 6 + [hbm],
-        out_specs=(vmem, vmem),
+    return pl.pallas_call(
+        functools.partial(layer_kernel, sp_count, tp_count, cap),
+        out_shape=jax.ShapeDtypeStruct((own, width), BF16),
+        in_specs=[hbm] * 11,
+        out_specs=pl.BlockSpec(memory_space=pltpu.VMEM),
         scratch_shapes=[
+            pltpu.VMEM(queries.shape, BF16),
+            pltpu.VMEM(key_value_pairs.shape, BF16),
+            pltpu.VMEM((heads, rows), F32),
+            pltpu.VMEM((own, width), BF16),
+            pltpu.VMEM((1, width), F32),
+            pltpu.VMEM((top, own), jnp.int32),
+            pltpu.VMEM((top, own), F32),
             pltpu.VMEM((sp_count, rows, key_value_pairs.shape[1]), BF16),
             pltpu.VMEM((sp_count, heads, rows), F32),
+            pltpu.VMEM((rows, heads), F32),
             pltpu.VMEM((heads, rows, 2 * HEAD_SIZE), BF16),
             pltpu.VMEM((heads, rows, 1), F32),
             pltpu.VMEM((heads, rows, 2 * HEAD_SIZE), F32),
@@ -525,45 +566,7 @@
             pltpu.VMEM((OUTER, own, width), F32),
             pltpu.VMEM((own, width), BF16),
             pltpu.VMEM((own, width), BF16),
-            dma,
-            dma((sp_count,)),
-            dma((sp_count,)),
-            dma((sp_count,)),
-            dma((sp_count,)),
-            dma((inner - 1,)),
-            dma((inner - 1,)),
-            dma,
-            dma,
-        ],
-        compiler_params=pltpu.CompilerParams(
-            collective_id=0, has_side_effects=True, vmem_limit_bytes=40 * 2**20
-        ),
-        name="mix",
-    )(
-        queries,
-        key_value_pairs,
-        forget_gate_total,
-        forget_gate_total.T,
-        residual_in,
-        norm_gain.reshape(1, -1),
-        out_weight,
-    )
-
-    top = routes.shape[1]
-    cap = max(2, 3 * own * top // (2 * sp_count))
-    cap = -(-cap // 8) * 8
-    flat = routes.reshape(-1)
-    order = jnp.arange(flat.shape[0], dtype=jnp.int32)
-    same = (flat[:, None] == flat[None, :]) & (order[None, :] < order[:, None])
-    slot = (flat * cap + jnp.sum(same.astype(jnp.int32), axis=1)).reshape(own, top)
-    ff = expert_gate.shape[2]
-    block = (cap, width)
-    return pl.pallas_call(
-        functools.partial(expert_kernel, sp_count, tp_count, cap),
-        out_shape=jax.ShapeDtypeStruct((own, width), BF16),
-        in_specs=[vmem] * 5 + [hbm] * 3,
-        out_specs=vmem,
-        scratch_shapes=[
+            pltpu.VMEM((own, width), F32),
             pltpu.VMEM((sp_count,) + block, BF16),
             pltpu.VMEM((sp_count, inner, OUTER) + block, BF16),
             pltpu.VMEM((width, ff), BF16),
@@ -575,28 +578,38 @@
             pltpu.VMEM((sp_count,) + block, BF16),
             pltpu.VMEM((sp_count,) + block, BF16),
             pltpu.VMEM((sp_count,) + block, BF16),
+            dma((8,)),
             dma((3,)),
+            some,
+            some,
+            some,
+            some,
+            dma((inner - 1,)),
+            dma((inner - 1,)),
             dma,
-            dma((sp_count,)),
-            dma((sp_count,)),
-            dma((sp_count,)),
-            dma((sp_count,)),
-            dma((inner - 1, sp_count)),
-            dma((inner - 1, sp_count)),
-            dma((inner - 1, sp_count)),
-            dma((inner - 1, sp_count)),
-            dma((inner - 1, sp_count)),
-            dma((inner - 1, sp_count)),
-            dma((sp_count,)),
-            dma((sp_count,)),
-            dma((sp_count,)),
-            dma((sp_count,)),
-        ],
+            dma,
+            dma,
+        ]
+        + [some] * 4
+        + [mate] * 6
+        + [some] * 4,
         compiler_params=pltpu.CompilerParams(
-            collective_id=1, has_side_effects=True, vmem_limit_bytes=60 * 2**20
+            collective_id=0, has_side_effects=True, vmem_limit_bytes=63 * 2**20
         ),
-        name="experts",
-    )(normed, hidden, slot, slot.T, route_weight, expert_gate, expert_up, expert_down)
+        name="layer",
+    )(
+        queries,
+        key_value_pairs,
+        forget_gate_total.T,
+        residual_in,
+        norm_gain.reshape(1, -1),
+        out_weight,
+        routes.T,
+        route_weight.T,
+        expert_gate,
+        expert_up,
+        expert_down,
+    )
 
 
 def solution(mesh):

time: 117 us -> 94.9 us (0.81)
  the two profiles are of different devices: /device:TPU:0 before, /device:TPU:13 now
where the time goes in v2:
time: 94.9 us; the launch traced here: 94.7 us
  Pallas kernels  93.1 us (98%)
  local copies, waits for them, and re-layouts  1.67 us (2%)
    pallas_call x1, Pallas kernels, local(): pl.pallas_call(functools.partial(layer_kernel, sp_count, tp_count, cap),...  93.1 us

profile of v2, /device:TPU:13, one launch (start us, length us, event | category | flops | bytes accessed | tf_op | source)
XLA Modules:
  0.0 94.7 jit_solution(8298222479138507351)
XLA Ops:
  0.0 93.1 %layer.1 = bf16[64,2048]{1,0:T(8,128)(2,1)} custom-call(bf16[256,512]{1,0:T(8,128)(2,1)} %q_hbm.1, bf16[256,128]{1,0:T(8,128)(2,1)} %kv_hbm.1, f32[8,256]{1,0:T(8,128)} %bitcast.4, bf16[64,2048]{1,0:T(8,128)(2,1)} %resid_hbm.1, f32[1,2048]{1,0:T(1,128)} %bitcast.5, bf16[512,2048]{1,0:T(8,128)(2,1)} %wout_hbm.1, s32[2,64]{1,0:T(2,128)} %bitcast.6, ...), custom_call_target="tpu_custom_call" | custom-call | tf_op jit(solution)/shard_map/layer/pallas_call | solution.py:543
  93.1 1.7 %copy.13 = bf16[64,2048]{1,0:T(8,128)(2,1)} copy(bf16[64,2048]{1,0:T(8,128)(2,1)} %layer.1) | data formatting | bytes 524288

commit v3 on v2

--- a/solution.py
+++ b/solution.py
@@ -435,34 +435,35 @@
             def _():
                 send_back(source, sp).start()
 
+    ahead_by = min(2, steps)
+
     def pipeline(i, carry):
-        @pl.when(i + 1 < steps)
+        @pl.when(i + ahead_by < steps)
         def _():
             for b in range(batch):
-                accept((i + 1) * batch + b)
+                accept((i + ahead_by) * batch + b)
 
         for b in range(batch):
             forward_across(at(i * batch + b))
-        ffn(i)
 
         @pl.when(i >= 1)
         def _():
             chip(i - 1)
 
-        @pl.when(i >= 2)
+        ffn(i)
+
+        @pl.when(i >= 1)
         def _():
-            give_back(i - 2)
-
-        return carry
-
-    for b in range(batch):
-        accept(b)
+            give_back(i - 1)
+
+        return carry
+
+    for step in range(ahead_by * batch):
+        accept(step)
     for load in loads:
         load.wait()
     lax.fori_loop(0, steps, pipeline, 0)
     chip(steps - 1)
-    if steps >= 2:
-        give_back(steps - 2)
     give_back(steps - 1)
     back[sp] = final[sp]
 

time: 94.9 us -> 94.6 us (level)
  the two profiles are of different devices: /device:TPU:13 before, /device:TPU:0 now
where the time goes in v3:
time: 94.6 us; the launch traced here: 94.4 us
  Pallas kernels  92.7 us (98%)
  local copies, waits for them, and re-layouts  1.67 us (2%)
    pallas_call x1, Pallas kernels, local(): pl.pallas_call(functools.partial(layer_kernel, sp_count, tp_count, cap),...  92.7 us

profile of v3, /device:TPU:0, one launch (start us, length us, event | category | flops | bytes accessed | tf_op | source)
XLA Modules:
  0.0 94.4 jit_solution(16218903470253844217)
XLA Ops:
  0.0 92.7 %layer.1 = bf16[64,2048]{1,0:T(8,128)(2,1)} custom-call(bf16[256,512]{1,0:T(8,128)(2,1)} %q_hbm.1, bf16[256,128]{1,0:T(8,128)(2,1)} %kv_hbm.1, f32[8,256]{1,0:T(8,128)} %bitcast.4, bf16[64,2048]{1,0:T(8,128)(2,1)} %resid_hbm.1, f32[1,2048]{1,0:T(1,128)} %bitcast.5, bf16[512,2048]{1,0:T(8,128)(2,1)} %wout_hbm.1, s32[2,64]{1,0:T(2,128)} %bitcast.6, ...), custom_call_target="tpu_custom_call" | custom-call | tf_op jit(solution)/shard_map/layer/pallas_call | solution.py:544
  92.7 1.7 %copy.13 = bf16[64,2048]{1,0:T(8,128)(2,1)} copy(bf16[64,2048]{1,0:T(8,128)(2,1)} %layer.1) | data formatting | bytes 524288
